TPU v7x, 32 devices: a whole 2x2x4 slice. The times are simulated.
32 devices in a mesh: fs: 16 (over z, y, x), tp: 2 (over core).
Axes of the slice: x: 2, y: 2, z: 4, core: 2. Of those that a mesh axis runs over, the one named last changes fastest.
Arguments:
- normed_input: bfloat16 [8192, 4096], P('fs', 'tp'), may hold values from -6 to 6
- value_cotangent: bfloat16 [8192, 2048], P('fs', 'tp'), may hold values from -0.01171875 to 0.01171875
- mixer_output: bfloat16 [8192, 2048], P('fs', 'tp'), may hold values from -6 to 6
- output_cotangent: bfloat16 [8192, 4096], P('fs', 'tp'), may hold values from -0.015625 to 0.015625
- value_factor: bfloat16 [4096, 128], replicated, may hold values from -0.5 to 0.5
- output_factor: bfloat16 [2048, 128], replicated, may hold values from -0.5 to 0.5
- value_master: float32 [4096, 2048], P('fs', 'tp'), may hold values from -0.09375 to 0.09375
- value_moment: float32 [128, 2048], P(None, 'tp'), may hold values from -6 to 6
- value_second: float32 [128, 2048], P(None, 'tp'), may hold values from 0.0625 to 16, as said below
- output_master: float32 [2048, 4096], P('fs', 'tp'), may hold values from -0.125 to 0.125
- output_moment: float32 [128, 4096], P(None, 'tp'), may hold values from -6 to 6
- output_second: float32 [128, 4096], P(None, 'tp'), may hold values from 0.0625 to 16, as said below
Outputs:
- value_step: float32 [4096, 2048], P('fs', 'tp')
- value_new: float32 [4096, 2048], P('fs', 'tp')
- value_copy: bfloat16 [4096, 2048], P(None, 'tp')
- value_moment_new: float32 [128, 2048], P(None, 'tp')
- value_second_new: float32 [128, 2048], P(None, 'tp')
- output_step: float32 [2048, 4096], P('fs', 'tp')
- output_new: float32 [2048, 4096], P('fs', 'tp')
- output_copy: bfloat16 [2048, 4096], P(None, 'tp')
- output_moment_new: float32 [128, 4096], P(None, 'tp')
- output_second_new: float32 [128, 4096], P(None, 'tp')
Inputs may be any that keep to these rules, and one draw needn't show every extreme that they name: `value_second`: positive, with a scale that differs between groups of columns. `output_second`: positive, with a scale that differs between groups of columns.
All inputs are finite; a program needn't handle non-finite values.
Results may differ from a plain program's by a relative error of at most 0.004.
Values may be sent and summed in bfloat16 or wider, within the bound.
A program may use at most 128 MiB of HBM per device.

v0:
```python
import jax
import jax.numpy as jnp
from jax import lax
from jax.sharding import PartitionSpec as P

D = 4096
WIDTH = 2048
R = 128
BETA_ONE = 0.8
BETA_TWO = 0.9
EPSILON = 1e-08
STEP_RATE = 0.005
FLOOR = 0.25


def contract_rows(left, right):
    return lax.dot_general(
        left.astype(jnp.float32),
        right.astype(jnp.float32),
        (((0,), (0,)), ((), ())),
        preferred_element_type=jnp.float32,
        precision=lax.Precision.HIGHEST,
    )


def moments(first, second, projected):
    first_new = BETA_ONE * first + (1.0 - BETA_ONE) * projected
    second_new = BETA_TWO * second + (1.0 - BETA_TWO) * projected * projected
    normalized = first_new / (jnp.sqrt(second_new) + EPSILON)
    return (first_new, second_new, normalized)


def per_device(
    normed_input,
    value_cotangent,
    mixer_output,
    output_cotangent,
    value_factor,
    output_factor,
    value_master,
    value_moment,
    value_second,
    output_master,
    output_moment,
    output_second,
):
    highest = lax.Precision.HIGHEST
    row_index = lax.axis_index("fs")
    column_index = lax.axis_index("tp")
    value_rows = value_master.shape[0]
    output_rows = output_master.shape[0]
    factor_here = lax.dynamic_slice_in_dim(
        value_factor, row_index * value_rows, value_rows, 0
    ).astype(jnp.float32)
    feature_cols = normed_input.shape[1]
    factor_features = lax.dynamic_slice_in_dim(
        value_factor, column_index * feature_cols, feature_cols, 0
    )
    input_partial = jnp.dot(normed_input, factor_features, preferred_element_type=jnp.float32)
    input_reduced = lax.psum(input_partial.astype(jnp.bfloat16), "tp").astype(jnp.float32)
    value_partial = contract_rows(input_reduced, value_cotangent)
    head_cols = mixer_output.shape[1]
    factor_heads = lax.dynamic_slice_in_dim(output_factor, column_index * head_cols, head_cols, 0)
    mixer_partial = jnp.dot(mixer_output, factor_heads, preferred_element_type=jnp.float32).astype(
        jnp.bfloat16
    )
    mixer_partial = lax.optimization_barrier(mixer_partial)
    mixer_reduced = lax.psum(mixer_partial.astype(jnp.float32).astype(jnp.bfloat16), "tp")
    output_partial = contract_rows(mixer_reduced, output_cotangent)
    value_projected, output_projected = lax.psum((value_partial, output_partial), "fs")
    value_moment_new, value_second_new, value_norm = moments(
        value_moment, value_second, value_projected
    )
    output_moment_new, output_second_new, output_norm = moments(
        output_moment, output_second, output_projected
    )
    value_total, output_total = lax.psum(
        (jnp.sum(value_norm * value_norm), jnp.sum(output_norm * output_norm)), "tp"
    )
    value_scale = lax.rsqrt(value_total / (R * WIDTH) + FLOOR)
    output_scale = lax.rsqrt(output_total / (R * D) + FLOOR)
    value_step = value_scale * jnp.dot(factor_here, value_norm, precision=highest)
    output_factor_rows = lax.dynamic_slice_in_dim(
        output_factor, row_index * output_rows, output_rows, 0
    ).astype(jnp.float32)
    output_step = output_scale * jnp.dot(output_factor_rows, output_norm, precision=highest)
    value_new = value_master - STEP_RATE * value_step
    output_new = output_master - STEP_RATE * output_step
    value_copy, output_copy = (
        lax.all_gather(value_new.astype(jnp.bfloat16), "fs", axis=0, tiled=True),
        lax.all_gather(output_new.astype(jnp.bfloat16), "fs", axis=0, tiled=True),
    )
    return (
        value_step,
        value_new,
        value_copy,
        value_moment_new,
        value_second_new,
        output_step,
        output_new,
        output_copy,
        output_moment_new,
        output_second_new,
    )


def solution(mesh):
    return jax.shard_map(
        per_device,
        mesh=mesh,
        in_specs=(
            P("fs", "tp"),
            P("fs", "tp"),
            P("fs", "tp"),
            P("fs", "tp"),
            P(),
            P(),
            P("fs", "tp"),
            P(None, "tp"),
            P(None, "tp"),
            P("fs", "tp"),
            P(None, "tp"),
            P(None, "tp"),
        ),
        out_specs=(
            P("fs", "tp"),
            P("fs", "tp"),
            P(None, "tp"),
            P(None, "tp"),
            P(None, "tp"),
            P("fs", "tp"),
            P("fs", "tp"),
            P(None, "tp"),
            P(None, "tp"),
            P(None, "tp"),
        ),
        check_vma=False,
    )
```

profile of v0, /device:TPU:0, one launch (start us, length us, event | category | flops | bytes accessed | tf_op | source)
XLA Modules:
  0.0 422.5 jit_solution(4155375352254664596)
XLA Ops:
  7.2 0.0 copy-start
  7.2 0.0 all-reduce.8.cloned.1.call-start
  7.2 0.0 copy-start.2
  7.3 2.6 fusion.1
  9.9 3.3 fusion
  13.1 0.0 all-reduce.8.cloned.1.call-update
  13.1 0.0 all-reduce.6.cloned.1.call-start
  13.2 21.1 %all-reduce.8.cloned.1.call-done = (bf16[512,128]{0,1:T(8,128)(2,1)}, bf16[512,128]{0,1:T(8,128)(2,1)}) async-done(((bf16[512,128]{0,1:T(8,128)(2,1)}, bf16[512,128]{0,1:T(8,128)(2,1)}), (bf16[512,128]{0,1:T(8,128)(2,1)}, bf16[512,128]{0,1:T(8,128)(2,1)})) %all-reduce.8.cloned.1.call-update) | async-done | bytes 262160 | tf_op jit(solution)/shard_map/psum | solution.py:60
  34.3 0.0 copy-done.2
  34.3 2.0 fusion.16
  36.3 0.0 copy-done
  36.3 0.0 copy-start.4
  36.3 2.4 fusion.17
  38.7 0.0 all-reduce.6.cloned.1.call-update
  38.8 0.0 all-gather.3.cloned.1.call-start
  38.8 121.2 %all-reduce.6.cloned.1.call-done = (f32[128,1024]{1,0:T(8,128)}, f32[128,2048]{1,0:T(8,128)}) async-done(((f32[128,1024]{1,0:T(8,128)}, f32[128,2048]{1,0:T(8,128)}), (f32[128,1024]{1,0:T(8,128)}, f32[128,2048]{1,0:T(8,128)})) %all-reduce.6.cloned.1.call-update) | async-done | bytes 1572880 | tf_op jit(solution)/shard_map/psum | solution.py:70
  160.0 0.0 copy-done.4
  160.0 0.0 copy-done.5
  160.0 3.0 multiply_reduce_fusion.1
  163.0 0.0 copy-done.3
  163.0 3.7 multiply_reduce_fusion
  166.8 3.1 all-reduce.1
  170.6 3.9 fusion.13
  174.4 0.0 all-gather.3.cloned.1.call-update
  174.5 0.0 all-gather.5.cloned.1.call-start
  175.2 0.0 copy-done.1
  175.2 4.2 fusion.12
  179.4 0.0 all-gather.5.cloned.1.call-update
  179.4 106.7 %all-gather.3.cloned.1.call-done = bf16[4096,1024]{1,0:T(8,128)(2,1)} async-done(((bf16[256,1024]{1,0:T(8,128)(2,1)}), bf16[4096,1024]{1,0:T(8,128)(2,1)}) %all-gather.3.cloned.1.call-update) | async-done | bytes 8388624 | tf_op jit(solution)/shard_map/all_gather | solution.py:90
  286.1 113.7 %all-gather.5.cloned.1.call-done = bf16[2048,2048]{1,0:T(8,128)(2,1)} async-done(((bf16[128,2048]{1,0:T(8,128)(2,1)}), bf16[2048,2048]{1,0:T(8,128)(2,1)}) %all-gather.5.cloned.1.call-update) | async-done | bytes 8388624 | tf_op jit(solution)/shard_map/all_gather | solution.py:91
  399.8 7.8 %copy.28 = bf16[4096,1024]{1,0:T(8,128)(2,1)} copy(bf16[4096,1024]{1,0:T(8,128)(2,1)} %all-gather.3.cloned.1.call-done) | data formatting | bytes 16777216
  407.5 8.4 %copy.29 = bf16[2048,2048]{1,0:T(8,128)(2,1)} copy(bf16[2048,2048]{1,0:T(8,128)(2,1)} %all-gather.5.cloned.1.call-done) | data formatting | bytes 16777216
  (3 shorter events, 0.0 us)
Async XLA Ops:
  7.2 29.1 %copy-start = (bf16[512,2048]{1,0:T(8,128)(2,1)S(1)}, bf16[512,2048]{1,0:T(8,128)(2,1)}, u32[]{:S(2)}) copy-start(bf16[512,2048]{1,0:T(8,128)(2,1)} %param.15) | copy-start | bytes 6291460
  7.2 27.1 %all-reduce.8.cloned.1.call-start = ((), (), s32[]{:S(2)}) async-start(), calls=%async_computation.3 | async-start | bytes 524288 | tf_op jit(solution)/shard_map/psum | solution.py:60
  7.2 27.1 %copy-start.2 = (bf16[512,1024]{1,0:T(8,128)(2,1)S(1)}, bf16[512,1024]{1,0:T(8,128)(2,1)}, u32[]{:S(2)}) copy-start(bf16[512,1024]{1,0:T(8,128)(2,1)} %param.13) | copy-start | bytes 3145732
  13.1 146.9 %all-reduce.6.cloned.1.call-start = ((), (), s32[]{:S(2)}) async-start(), calls=%async_computation.2 | async-start | bytes 3145728 | tf_op jit(solution)/shard_map/psum | solution.py:70
  36.3 123.7 %copy-start.4 = (f32[128,1024]{1,0:T(8,128)S(1)}, f32[128,1024]{1,0:T(8,128)}, u32[]{:S(2)}) copy-start(f32[128,1024]{1,0:T(8,128)} %param.20) | copy-start | bytes 1572868
  36.3 123.7 %copy-start.5 = (f32[128,1024]{1,0:T(8,128)S(1)}, f32[128,1024]{1,0:T(8,128)}, u32[]{:S(2)}) copy-start(f32[128,1024]{1,0:T(8,128)} %param.19) | copy-start | bytes 1572868
  38.8 247.3 %all-gather.3.cloned.1.call-start = ((), (), s32[]{:S(2)}) async-start(), calls=%async_computation | async-start | bytes 8912896 | tf_op jit(solution)/shard_map/all_gather | solution.py:90
  160.0 3.0 copy-start.3
  166.8 8.4 %copy-start.1 = (f32[128,2048]{1,0:T(8,128)}, f32[128,2048]{1,0:T(8,128)S(1)}, u32[]{:S(2)}) copy-start(f32[128,2048]{1,0:T(8,128)S(1)} %get-tuple-element.47) | copy-start | bytes 3145732
  174.5 225.3 %all-gather.5.cloned.1.call-start = ((), (), s32[]{:S(2)}) async-start(), calls=%async_computation.1 | async-start | bytes 8912896 | tf_op jit(solution)/shard_map/all_gather | solution.py:91
Sparse Core Ops, SparseCore 0:
  13.3 21.0 all-reduce.7
  41.1 118.9 all-reduce.5
  174.6 111.4 all-gather.2
  289.3 110.4 all-gather.4
where the time goes:
time: 423 us
  waiting for transfers between devices  363 us (86%)
  matrix products  18.3 us (4%)
  local copies, waits for them, and re-layouts  16.2 us (4%)
  between operations  15.2 us (4%)
  other arithmetic  6.75 us (2%)
    psum x1, waiting for transfers between devices, per_device(): lax.psum((value_partial, output_partial), 'fs')  121 us
    all_gather x1, waiting for transfers between devices, per_device(): lax.all_gather(output_new.astype(jnp.bfloat16), 'fs', axis=0, tiled=True)  114 us
    all_gather x1, waiting for transfers between devices, per_device(): lax.all_gather(value_new.astype(jnp.bfloat16), 'fs', axis=0, tiled=True)  107 us
    psum x1, waiting for transfers between devices, per_device(): lax.psum(input_partial.astype(jnp.bfloat16), 'tp').astype(jnp.float32)  21.1 us
    unnamed x14, local copies, waits for them, and re-layouts  16.2 us
  transfers between devices with their start and end apart: 4, of which 4 were waited for; matrix products, arithmetic and copies ran while one was open for 1% of the time, Pallas kernels for 0%

commit v1 on v0

--- a/solution.py
+++ b/solution.py
@@ -57,7 +57,9 @@
         value_factor, column_index * feature_cols, feature_cols, 0
     )
     input_partial = jnp.dot(normed_input, factor_features, preferred_element_type=jnp.float32)
-    input_reduced = lax.psum(input_partial.astype(jnp.bfloat16), "tp").astype(jnp.float32)
+    input_reduced = jnp.sum(
+        lax.all_gather(input_partial.astype(jnp.bfloat16), "tp"), axis=0
+    ).astype(jnp.float32)
     value_partial = contract_rows(input_reduced, value_cotangent)
     head_cols = mixer_output.shape[1]
     factor_heads = lax.dynamic_slice_in_dim(output_factor, column_index * head_cols, head_cols, 0)

time: 423 us -> 420 us (level)
  waiting for transfers between devices: 363 us -> 357 us
    psum x1, waiting for transfers between devices: 21.1 us -> 13.7 us  [per_device(): lax.psum(mixer_partial.astype(jnp.float32).astype(jnp.bfloat16), 'tp')]
    unnamed x14 -> x12, local copies, waits for them, and re-layouts: 16.2 us -> 16.2 us
  transfers between devices with their start and end apart: 4 -> 4, of which waited for: 4 -> 4; matrix products, arithmetic and copies ran while one was open for 1% -> 2% of each run, Pallas kernels for 0% -> 0%
where the time goes in v1:
time: 420 us
  waiting for transfers between devices  357 us (85%)
  matrix products  17.9 us (4%)
  local copies, waits for them, and re-layouts  16.4 us (4%)
  between operations  15.2 us (4%)
  other arithmetic  7.42 us (2%)
  blocking collectives  5.21 us (1%)
    psum x1, waiting for transfers between devices, per_device(): lax.psum((value_partial, output_partial), 'fs')  123 us
    all_gather x1, waiting for transfers between devices, per_device(): lax.all_gather(output_new.astype(jnp.bfloat16), 'fs', axis=0, tiled=True)  114 us
    all_gather x1, waiting for transfers between devices, per_device(): lax.all_gather(value_new.astype(jnp.bfloat16), 'fs', axis=0, tiled=True)  107 us
    unnamed x12, local copies, waits for them, and re-layouts  16.2 us
    psum x1, waiting for transfers between devices, per_device(): lax.psum(mixer_partial.astype(jnp.float32).astype(jnp.bfloat16), 'tp')  13.7 us
  transfers between devices with their start and end apart: 4, of which 4 were waited for; matrix products, arithmetic and copies ran while one was open for 2% of the time, Pallas kernels for 0%

profile of v1, /device:TPU:0, one launch (start us, length us, event | category | flops | bytes accessed | tf_op | source)
XLA Modules:
  0.0 419.8 jit_solution(6633452624262869503)
XLA Ops:
  7.2 0.0 copy-start
  7.2 0.0 all-reduce.5.cloned.1.call-start
  7.2 2.6 fusion.1
  9.8 0.0 all-reduce.5.cloned.1.call-update
  9.9 0.0 all-reduce.7.cloned.1.call-start
  9.9 2.6 fusion
  12.5 2.1 all-gather
  14.6 0.2 reshape.20
  14.8 0.7 reduce_sum.30
  15.5 2.3 fusion.16
  17.8 13.7 %all-reduce.5.cloned.1.call-done = bf16[512,128]{0,1:T(8,128)(2,1)} async-done(((bf16[512,128]{0,1:T(8,128)(2,1)}), bf16[512,128]{0,1:T(8,128)(2,1)}) %all-reduce.5.cloned.1.call-update) | async-done | bytes 131088 | tf_op jit(solution)/shard_map/psum | solution.py:70
  31.6 0.0 copy-done
  31.6 2.3 fusion.17
  33.9 0.0 all-reduce.7.cloned.1.call-update
  33.9 0.0 all-gather.4.cloned.1.call-start
  34.0 123.3 %all-reduce.7.cloned.1.call-done = (f32[128,1024]{1,0:T(8,128)}, f32[128,2048]{1,0:T(8,128)}) async-done(((f32[128,1024]{1,0:T(8,128)}, f32[128,2048]{1,0:T(8,128)}), (f32[128,1024]{1,0:T(8,128)}, f32[128,2048]{1,0:T(8,128)})) %all-reduce.7.cloned.1.call-update) | async-done | bytes 1572880 | tf_op jit(solution)/shard_map/psum | solution.py:72
  157.3 0.0 copy-done.3
  157.3 0.0 copy-done.4
  157.3 3.0 multiply_reduce_fusion.1
  160.3 0.0 copy-done.2
  160.3 3.7 multiply_reduce_fusion
  164.0 3.1 all-reduce.1
  167.8 3.9 fusion.13
  171.7 0.0 all-gather.4.cloned.1.call-update
  171.7 0.0 all-gather.6.cloned.1.call-start
  172.5 0.0 copy-done.1
  172.5 4.2 fusion.12
  176.6 0.0 all-gather.6.cloned.1.call-update
  176.7 106.7 %all-gather.4.cloned.1.call-done = bf16[4096,1024]{1,0:T(8,128)(2,1)} async-done(((bf16[256,1024]{1,0:T(8,128)(2,1)}), bf16[4096,1024]{1,0:T(8,128)(2,1)}) %all-gather.4.cloned.1.call-update) | async-done | bytes 8388624 | tf_op jit(solution)/shard_map/all_gather | solution.py:92
  283.3 113.7 %all-gather.6.cloned.1.call-done = bf16[2048,2048]{1,0:T(8,128)(2,1)} async-done(((bf16[128,2048]{1,0:T(8,128)(2,1)}), bf16[2048,2048]{1,0:T(8,128)(2,1)}) %all-gather.6.cloned.1.call-update) | async-done | bytes 8388624 | tf_op jit(solution)/shard_map/all_gather | solution.py:93
  397.0 7.8 %copy.27 = bf16[4096,1024]{1,0:T(8,128)(2,1)} copy(bf16[4096,1024]{1,0:T(8,128)(2,1)} %all-gather.4.cloned.1.call-done) | data formatting | bytes 16777216
  404.8 8.4 %copy.28 = bf16[2048,2048]{1,0:T(8,128)(2,1)} copy(bf16[2048,2048]{1,0:T(8,128)(2,1)} %all-gather.6.cloned.1.call-done) | data formatting | bytes 16777216
  (4 shorter events, 0.0 us)
Async XLA Ops:
  7.2 24.4 %copy-start = (bf16[512,2048]{1,0:T(8,128)(2,1)S(1)}, bf16[512,2048]{1,0:T(8,128)(2,1)}, u32[]{:S(2)}) copy-start(bf16[512,2048]{1,0:T(8,128)(2,1)} %param.15) | copy-start | bytes 6291460
  7.2 24.4 %all-reduce.5.cloned.1.call-start = ((), (), s32[]{:S(2)}) async-start(), calls=%async_computation.1 | async-start | bytes 262144 | tf_op jit(solution)/shard_map/psum | solution.py:70
  9.9 147.4 %all-reduce.7.cloned.1.call-start = ((), (), s32[]{:S(2)}) async-start(), calls=%async_computation.3 | async-start | bytes 3145728 | tf_op jit(solution)/shard_map/psum | solution.py:72
  17.8 139.4 %copy-start.3 = (f32[128,1024]{1,0:T(8,128)S(1)}, f32[128,1024]{1,0:T(8,128)}, u32[]{:S(2)}) copy-start(f32[128,1024]{1,0:T(8,128)} %param.20) | copy-start | bytes 1572868
  17.8 139.4 %copy-start.4 = (f32[128,1024]{1,0:T(8,128)S(1)}, f32[128,1024]{1,0:T(8,128)}, u32[]{:S(2)}) copy-start(f32[128,1024]{1,0:T(8,128)} %param.19) | copy-start | bytes 1572868
  33.9 249.4 %all-gather.4.cloned.1.call-start = ((), (), s32[]{:S(2)}) async-start(), calls=%async_computation | async-start | bytes 8912896 | tf_op jit(solution)/shard_map/all_gather | solution.py:92
  157.3 3.0 copy-start.2
  164.0 8.4 %copy-start.1 = (f32[128,2048]{1,0:T(8,128)}, f32[128,2048]{1,0:T(8,128)S(1)}, u32[]{:S(2)}) copy-start(f32[128,2048]{1,0:T(8,128)S(1)} %get-tuple-element.45) | copy-start | bytes 3145732
  171.7 225.3 %all-gather.6.cloned.1.call-start = ((), (), s32[]{:S(2)}) async-start(), calls=%async_computation.2 | async-start | bytes 8912896 | tf_op jit(solution)/shard_map/all_gather | solution.py:93
Sparse Core Ops, SparseCore 0:
  10.9 20.6 all-reduce.4
  38.3 118.9 all-reduce.6
  171.8 111.4 all-gather.3
  286.5 110.4 all-gather.5
